TPU v7x, 32 devices: a whole 2x2x4 slice. The times are simulated.
32 devices in a mesh: dp: 4 (over y, x), kv: 4 (over z), tp: 2 (over core).
Axes of the slice: x: 2, y: 2, z: 4, core: 2. Of those that a mesh axis runs over, the one named last changes fastest.
Arguments:
- tokens: bfloat16 [128, 2048], P('dp', ('kv', 'tp')), may hold values from -100 to 100
- delta_state: float32 [128, 8, 128, 128], P(('dp', 'kv'), 'tp'), may hold values from -0.6 to 0.6
- gain_in: bfloat16 [2048], P('kv'), may hold values from 0.099609375 to 1.8984375
- w_query: bfloat16 [2048, 1024], P('kv', 'tp'), may hold values from -0.125 to 0.125
- w_key: bfloat16 [2048, 1024], P('kv', 'tp'), may hold values from -0.125 to 0.125
- w_value: bfloat16 [2048, 1024], P('kv', 'tp'), may hold values from -0.125 to 0.125
- w_out_gate: bfloat16 [2048, 1024], P('kv', 'tp'), may hold values from -0.125 to 0.125
- w_beta: bfloat16 [2048, 8], P('kv'), may hold values from -0.125 to 0.125
- w_decay: bfloat16 [2048, 8], P('kv'), may hold values from -0.125 to 0.125
- decay_rate: float32 [8], P('tp'), may hold values from 0.05 to 3
- head_gain: float32 [128], replicated, may hold values from 0.1 to 1.9
- w_mix: bfloat16 [1024, 2048], P('tp', 'kv'), may hold values from -0.1875 to 0.1875
- gain_mid: bfloat16 [2048], P('kv'), may hold values from 0.099609375 to 1.8984375
- w_gate: bfloat16 [2048, 5632], P('tp', 'kv'), may hold values from -0.125 to 0.125
- w_up: bfloat16 [2048, 5632], P('tp', 'kv'), may hold values from -0.125 to 0.125
- w_down: bfloat16 [5632, 2048], P('kv', 'tp'), may hold values from -0.078125 to 0.078125
Outputs:
- layer_out: bfloat16 [128, 2048], P('dp', ('kv', 'tp'))
- next_state: float32 [128, 8, 128, 128], P(('dp', 'kv'), 'tp')
All inputs are finite; a program needn't handle non-finite values.
Results may differ from a plain program's by a relative error of at most 0.0095.
Values may be sent and summed in bfloat16 or wider, within the bound.
A program may use at most 64 MiB of HBM per device.

v0:
```python
import jax
import jax.numpy as jnp
from jax import lax
from jax.sharding import PartitionSpec as P

D = 2048
HEAD_DIM = 128
norm_epsilon = 1e-06


def unit_rows(vector):
    return vector * lax.rsqrt(jnp.sum(vector * vector, axis=-1, keepdims=True) + norm_epsilon)


def mixer_core(
    query_lin, key_lin, value_lin, gate_lin, beta_lin, decay_lin, delta_state, decay_rate, head_gain
):
    seq_count = query_lin.shape[0]
    head_count = beta_lin.shape[1]
    shaped = lambda matrix: matrix.reshape(seq_count, head_count, HEAD_DIM)
    query = unit_rows(jax.nn.silu(shaped(query_lin))) * HEAD_DIM ** (-0.5)
    key_vec = unit_rows(jax.nn.silu(shaped(key_lin)))
    value_vec = jax.nn.silu(shaped(value_lin))
    write_rate = jax.nn.sigmoid(beta_lin)
    keep_rate = jnp.exp(-decay_rate[None, :] * jax.nn.softplus(decay_lin))
    recalled = jnp.einsum("bhkv,bhk->bhv", delta_state, key_vec, precision=lax.Precision.HIGHEST)
    correction = write_rate[..., None] * (value_vec - keep_rate[..., None] * recalled)
    next_state = (
        keep_rate[..., None, None] * delta_state + key_vec[..., :, None] * correction[..., None, :]
    )
    readout = jnp.einsum("bhkv,bhk->bhv", next_state, query, precision=lax.Precision.HIGHEST)
    readout = readout * lax.rsqrt(
        jnp.mean(readout * readout, axis=-1, keepdims=True) + norm_epsilon
    )
    readout = readout * head_gain * jax.nn.silu(shaped(gate_lin))
    return (readout.reshape(seq_count, head_count * HEAD_DIM).astype(jnp.bfloat16), next_state)


def local(
    tokens,
    delta_state,
    gain_in,
    w_query,
    w_key,
    w_value,
    w_out_gate,
    w_beta,
    w_decay,
    decay_rate,
    head_gain,
    w_mix,
    gain_mid,
    w_gate,
    w_up,
    w_down,
):
    group_size = lax.axis_size("kv")
    group_pos = lax.axis_index("kv")
    core_pos = lax.axis_index("tp")
    all_rows = tokens.shape[0]
    own_rows = all_rows // group_size
    own_first = group_pos * own_rows
    feature_count = tokens.shape[1]
    head_count = w_query.shape[1] // HEAD_DIM
    width_dev = w_query.shape[1]
    token_float = tokens.astype(jnp.float32)
    sum_squares = jnp.sum(token_float * token_float, axis=1, keepdims=True)
    whole_rows, square_pair = (
        lax.all_gather(tokens, "tp", axis=1, tiled=True),
        lax.all_gather(sum_squares.astype(jnp.bfloat16), "tp", axis=1, tiled=True).astype(
            sum_squares.dtype
        ),
    )
    square_total = lax.psum(jnp.sum(square_pair, axis=1), "kv")
    row_scale = lax.rsqrt(square_total / D + norm_epsilon)
    normed = (whole_rows.astype(jnp.float32) * gain_in.astype(jnp.float32)).astype(jnp.bfloat16)
    beta_cols = lax.dynamic_slice_in_dim(w_beta, core_pos * head_count, head_count, 1)
    decay_cols = lax.dynamic_slice_in_dim(w_decay, core_pos * head_count, head_count, 1)
    row_block = normed
    results = [
        jnp.dot(row_block, weight, preferred_element_type=jnp.float32)
        for weight in (w_query, w_key, w_value, w_out_gate, beta_cols, decay_cols)
    ]
    summand = jnp.concatenate(results, axis=1)
    projected = lax.psum_scatter(
        summand.astype(jnp.bfloat16), "kv", scatter_dimension=0, tiled=True
    ).astype(jnp.float32)
    projected = projected * lax.dynamic_slice_in_dim(row_scale, own_first, own_rows, 0)[:, None]
    mixed, next_state = mixer_core(
        projected[:, :width_dev],
        projected[:, width_dev : 2 * width_dev],
        projected[:, 2 * width_dev : 3 * width_dev],
        projected[:, 3 * width_dev : 4 * width_dev],
        projected[:, 4 * width_dev : 4 * width_dev + head_count],
        projected[:, 4 * width_dev + head_count :],
        delta_state,
        decay_rate,
        head_gain,
    )
    attn_part = jnp.dot(
        lax.all_gather(mixed, "kv", axis=0, tiled=True), w_mix, preferred_element_type=jnp.float32
    )
    attn = lax.psum_scatter(
        attn_part.astype(jnp.bfloat16), "tp", scatter_dimension=1, tiled=True
    ).astype(jnp.float32)
    middle_own = (token_float + attn).astype(jnp.bfloat16)
    middle_float = middle_own.astype(jnp.float32)
    mid_squares = jnp.sum(middle_float * middle_float, axis=1, keepdims=True)
    gain_own = lax.dynamic_slice_in_dim(gain_mid, core_pos * feature_count, feature_count, 0)
    normed_own = (middle_float * gain_own.astype(jnp.float32)).astype(jnp.bfloat16)
    normed_half, square_parts = (
        lax.all_gather(normed_own, "kv", axis=1, tiled=True),
        lax.all_gather(mid_squares.astype(jnp.bfloat16), "kv", axis=1, tiled=True).astype(
            mid_squares.dtype
        ),
    )
    mid_total = lax.psum(jnp.sum(square_parts, axis=1), "tp")
    mid_scale = lax.rsqrt(mid_total / D + norm_epsilon)
    hidden_dev = w_gate.shape[1]
    row_block = normed_half
    summand = jnp.concatenate(
        [
            jnp.dot(row_block, w_gate, preferred_element_type=jnp.float32),
            jnp.dot(row_block, w_up, preferred_element_type=jnp.float32),
        ],
        axis=1,
    )
    gate_up = lax.psum(summand.astype(jnp.bfloat16), "tp").astype(jnp.float32)
    gate_up = gate_up * mid_scale[:, None]
    activated = (jax.nn.silu(gate_up[:, :hidden_dev]) * gate_up[:, hidden_dev:]).astype(
        jnp.bfloat16
    )
    down_local = jnp.dot(activated, w_down, preferred_element_type=jnp.float32)
    down_part = lax.psum_scatter(
        down_local.astype(jnp.bfloat16), "kv", scatter_dimension=1, tiled=True
    ).astype(jnp.float32)
    layer_out = (middle_float + down_part).astype(jnp.bfloat16)
    return (layer_out, next_state)


def solution(mesh):
    in_specs = (
        P("dp", ("kv", "tp")),
        P(("dp", "kv"), "tp", None, None),
        P("kv"),
        P("kv", "tp"),
        P("kv", "tp"),
        P("kv", "tp"),
        P("kv", "tp"),
        P("kv", None),
        P("kv", None),
        P("tp"),
        P(),
        P("tp", "kv"),
        P("kv"),
        P("tp", "kv"),
        P("tp", "kv"),
        P("kv", "tp"),
    )
    out_specs = (P("dp", ("kv", "tp")), P(("dp", "kv"), "tp", None, None))
    return jax.shard_map(local, mesh=mesh, in_specs=in_specs, out_specs=out_specs, check_vma=False)
```

profile of v0, /device:TPU:0, one launch (start us, length us, event | category | flops | bytes accessed | tf_op | source)
XLA Modules:
  0.0 164.7 jit_solution(10898741676465725415)
XLA Ops:
  7.3 0.8 convert_element_type.92
  8.1 2.3 %all_gather.15 = bf16[32,512]{1,0:T(8,128)(2,1)S(1)} all-gather(bf16[32,256]{1,0:T(8,128)(2,1)} %param.16), channel_id=1, replica_groups=mesh['dp'=4,'kv'=4,'tp'=2] {'tp'}, dimensions={1}, use_global_device_ids=true | all-gather | bytes 49152 | tf_op jit(solution)/shard_map/all_gather | solution.py:69
  12.3 1.2 convolution_convert_fusion.6
  13.5 1.2 convolution_convert_fusion.5
  14.7 1.2 convolution_convert_fusion.4
  16.0 1.2 convolution_convert_fusion.7
  18.2 1.8 %all-gather = bf16[2,1,32]{2,1,0:T(2,128)(2,1)S(1)} all-gather(bf16[1,1,32]{2,1,0:T(2,128)(2,1)S(1)} %bitcast.72), channel_id=1, replica_groups=mesh['dp'=4,'kv'=4,'tp'=2] {'tp'}, dimensions={0}, use_global_device_ids=true | all-gather | bytes 192 | tf_op jit(solution)/shard_map/all_gather | solution.py:70
  20.0 13.3 %psum.21 = f32[32]{0:T(128)S(1)} all-reduce(f32[32]{0:T(128)S(1)} %convert_reduce_fusion.1), channel_id=1, replica_groups=mesh['dp'=4,'kv'=4,'tp'=2] {'kv'}, use_global_device_ids=true, to_apply=%region_3.0 | all-reduce | flops 32 | bytes 256 | tf_op jit(solution)/shard_map/psum | solution.py:74
  34.7 20.7 %all-reduce.6.cloned.1.call-done = bf16[32,2056]{1,0:T(8,128)(2,1)} async-done(((bf16[32,2056]{1,0:T(8,128)(2,1)}), bf16[32,2056]{1,0:T(8,128)(2,1)}) %all-reduce.6.cloned.1.call-update) | async-done | bytes 131600
  55.4 0.8 convert_multiply_fusion.1
  56.7 3.6 %fusion.16 = f32[8,4,1,128]{3,2,1,0:T(1,128)S(1)} fusion(f32[8,4,128,128]{3,2,1,0:T(8,128)} %param.17, f32[8,4,128,1]{2,0,1,3:T(8,128)S(1)} %bitcast.70), kind=kOutput, calls=%fused_computation.43 | convolution fusion | flops 6291456 | bytes 2129920 | tf_op jit(solution)/shard_map/bhkv,bhk->bhv/dot_general | solution.py:26
  61.1 1.3 copy-done.2
  62.4 1.9 %fusion.14 = f32[8,4,1,128]{3,2,1,0:T(1,128)S(1)} fusion(f32[8,4,128,128]{3,2,1,0:T(8,128)S(1)} %multiply_add_fusion, f32[8,4,128,1]{2,0,1,3:T(8,128)S(1)} %get-tuple-element.4), kind=kOutput, calls=%fused_computation.41 | convolution fusion | flops 6291456 | bytes 2129920 | tf_op jit(solution)/shard_map/bhkv,bhk->bhv/dot_general | solution.py:31
  64.5 13.1 %all_gather.17 = bf16[32,512]{1,0:T(8,128)(2,1)S(1)} all-gather(bf16[8,512]{1,0:T(8,128)(2,1)S(1)} %fusion.18), channel_id=1, replica_groups=mesh['dp'=4,'kv'=4,'tp'=2] {'kv'}, dimensions={0}, use_global_device_ids=true | all-gather | bytes 40960 | tf_op jit(solution)/shard_map/all_gather | solution.py:101
  78.6 7.6 %reduce-scatter.3.cloned.1.call-done = bf16[32,256]{1,0:T(8,128)(2,1)} async-done(((bf16[32,512]{1,0:T(8,128)(2,1)}), bf16[32,256]{1,0:T(8,128)(2,1)}) %reduce-scatter.3.cloned.1.call-update) | async-done | bytes 16400 | tf_op jit(solution)/shard_map/reduce_scatter | solution.py:103
  86.2 0.8 fusion.6
  87.0 11.1 %all-gather.1 = bf16[4,1,32]{2,1,0:T(2,128)(2,1)S(1)} all-gather(bf16[1,1,32]{2,1,0:T(2,128)(2,1)S(1)} %bitcast.71), channel_id=1, replica_groups=mesh['dp'=4,'kv'=4,'tp'=2] {'kv'}, dimensions={0}, use_global_device_ids=true | all-gather | bytes 320 | tf_op jit(solution)/shard_map/all_gather | solution.py:113
  98.1 2.5 %psum.23 = f32[32]{0:T(128)S(1)} all-reduce(f32[32]{0:T(128)S(1)} %convert_reduce_fusion), channel_id=1, replica_groups=mesh['dp'=4,'kv'=4,'tp'=2] {'tp'}, use_global_device_ids=true, to_apply=%region_11.12 | all-reduce | flops 32 | bytes 256 | tf_op jit(solution)/shard_map/psum | solution.py:117
  100.6 13.2 %all_gather.18 = bf16[32,1024]{1,0:T(8,128)(2,1)S(1)} all-gather(bf16[32,256]{1,0:T(8,128)(2,1)S(1)} %get-tuple-element.9), channel_id=1, replica_groups=mesh['dp'=4,'kv'=4,'tp'=2] {'kv'}, dimensions={1}, use_global_device_ids=true | all-gather | bytes 81920 | tf_op jit(solution)/shard_map/all_gather | solution.py:112
  115.8 16.3 %all-reduce.4.cloned.1.call-done = bf16[32,2816]{1,0:T(8,128)(2,1)} async-done(((bf16[32,2816]{1,0:T(8,128)(2,1)}), bf16[32,2816]{1,0:T(8,128)(2,1)}) %all-reduce.4.cloned.1.call-update) | async-done | bytes 180240 | tf_op jit(solution)/shard_map/psum | solution.py:128
  132.1 1.0 convert_multiply_fusion
  133.1 3.0 %convolution_convert_fusion.2 = bf16[32,1024]{1,0:T(8,128)(2,1)} fusion(bf16[1408,1024]{1,0:T(8,128)(2,1)} %param.31, f32[32,2816]{1,0:T(8,128)S(1)} %convert_multiply_fusion), kind=kOutput, calls=%fused_computation.3 | convolution fusion | flops 92577792 | bytes 3309568 | tf_op jit(solution)/shard_map/dot_general | solution.py:133
  136.2 20.7 %reduce-scatter.5.cloned.1.call-done = bf16[32,256]{1,0:T(8,128)(2,1)} async-done(((bf16[32,1024]{1,0:T(8,128)(2,1)}), bf16[32,256]{1,0:T(8,128)(2,1)}) %reduce-scatter.5.cloned.1.call-update) | async-done | bytes 16400 | tf_op jit(solution)/shard_map/reduce_scatter | solution.py:134
  156.8 1.3 fusion.7
  (60 shorter events, 7.9 us)
Async XLA Ops:
  7.2 106.7 %copy-start = (bf16[1024,1408]{1,0:T(8,128)(2,1)S(1)}, bf16[1024,1408]{1,0:T(8,128)(2,1)}, u32[]{:S(2)}) copy-start(bf16[1024,1408]{1,0:T(8,128)(2,1)} %param.30) | copy-start | bytes 8650756
  7.2 26.2 %copy-start.10 = (u32[32]{0:T(128)S(1)}, u32[32]{0:T(128)}, u32[]{:S(2)}) copy-start(u32[32]{0:T(128)} %constant.48) | copy-start | bytes 388
  7.2 10.9 %copy-start.5 = (bf16[32,256]{1,0:T(8,128)(2,1)S(1)}, bf16[32,256]{1,0:T(8,128)(2,1)}, u32[]{:S(2)}) copy-start(bf16[32,256]{1,0:T(8,128)(2,1)} %param.16) | copy-start | bytes 49156
  7.2 11.0 %copy-start.9 = (f32[4]{0:T(128)S(1)}, f32[4]{0:T(128)}, u32[]{:S(2)}) copy-start(f32[4]{0:T(128)} %param.25) | copy-start | bytes 52
  7.2 48.2 %all-reduce.6.cloned.1.call-start = ((), (), s32[]{:S(2)}) async-start(), calls=%async_computation.5 | async-start | bytes 278528
  18.0 68.2 %reduce-scatter.3.cloned.1.call-start = ((), (), s32[]{:S(2)}) async-start(), calls=%async_computation.2 | async-start | bytes 49152 | tf_op jit(solution)/shard_map/reduce_scatter | solution.py:103
  56.6 3.8 %copy-start.1 = (f32[8,4,128,128]{3,2,1,0:T(8,128)S(1)}, f32[8,4,128,128]{3,2,1,0:T(8,128)}, u32[]{:S(2)}) copy-start(f32[8,4,128,128]{3,2,1,0:T(8,128)} %param.17) | copy-start | bytes 6291460
  61.1 1.3 copy-start.2
  61.1 3.3 %copy-start.7 = (f32[128]{0:T(128)S(1)}, f32[128]{0:T(128)}, u32[]{:S(2)}) copy-start(f32[128]{0:T(128)} %param.26) | copy-start | bytes 1540
  61.1 16.5 %copy-start.4 = (bf16[512,512]{1,0:T(8,128)(2,1)S(1)}, bf16[512,512]{1,0:T(8,128)(2,1)}, u32[]{:S(2)}) copy-start(bf16[512,512]{1,0:T(8,128)(2,1)} %param.27) | copy-start | bytes 1572868
  61.1 17.4 %copy-start.8 = (bf16[512]{0:T(512)(128)(2,1)S(1)}, bf16[512]{0:T(512)(128)(2,1)}, u32[]{:S(2)}) copy-start(bf16[512]{0:T(512)(128)(2,1)} %param.28) | copy-start | bytes 3076
  78.5 53.7 %all-reduce.4.cloned.1.call-start = ((), (), s32[]{:S(2)}) async-start(), calls=%async_computation.3 | async-start | bytes 360448 | tf_op jit(solution)/shard_map/psum | solution.py:128
  100.6 13.8 %copy-start.3 = (bf16[1024,1408]{1,0:T(8,128)(2,1)S(1)}, bf16[1024,1408]{1,0:T(8,128)(2,1)}, u32[]{:S(2)}) copy-start(bf16[1024,1408]{1,0:T(8,128)(2,1)} %param.29) | copy-start | bytes 8650756
  115.0 41.8 %copy-start.6 = (bf16[32,256]{1,0:T(8,128)(2,1)S(1)}, bf16[32,256]{1,0:T(8,128)(2,1)}, u32[]{:S(2)}) copy-start(bf16[32,256]{1,0:T(8,128)(2,1)} %reduce-scatter.3.cloned.1.call-done) | copy-start | bytes 49156
  115.7 41.1 %reduce-scatter.5.cloned.1.call-start = ((), (), s32[]{:S(2)}) async-start(), calls=%async_computation.4 | async-start | bytes 81920 | tf_op jit(solution)/shard_map/reduce_scatter | solution.py:134
Sparse Core Ops, SparseCore 0:
  18.1 37.2 all-reduce.5
  78.6 7.5 reduce-scatter.2
  115.9 16.1 all-reduce.3
  136.3 20.4 reduce-scatter.4
where the time goes:
time: 165 us
  waiting for transfers between devices  65.3 us (40%)
  blocking collectives  57.3 us (35%)
  matrix products  17 us (10%)
  between operations  14.6 us (9%)
  other arithmetic  7.06 us (4%)
  local copies, waits for them, and re-layouts  3.14 us (2%)
    unnamed x5, waiting for transfers between devices  20.8 us
    reduce_scatter x1, waiting for transfers between devices, local(): lax.psum_scatter(down_local.astype(jnp.bfloat16), 'kv', scatter_dimension...  20.7 us
    psum x1, waiting for transfers between devices, local(): gate_up = lax.psum(summand.astype(jnp.bfloat16), 'tp').astype(jnp.float32)  16.3 us
    psum x1, blocking collectives, local(): square_total = lax.psum(jnp.sum(square_pair, axis=1), 'kv')  13.3 us
    all_gather x1, blocking collectives, local(): lax.all_gather(normed_own, 'kv', axis=1, tiled=True)  13.2 us
    all_gather x1, blocking collectives, local(): lax.all_gather(mixed, 'kv', axis=0, tiled=True)  13.1 us
    all_gather x1, blocking collectives, local(): lax.all_gather(mid_squares.astype(jnp.bfloat16), 'kv', axis=1, tiled=True)  11.1 us
    reduce_scatter x1, waiting for transfers between devices, local(): lax.psum_scatter(attn_part.astype(jnp.bfloat16), 'tp', scatter_dimension=...  7.59 us
  transfers between devices with their start and end apart: 4, of which 4 were waited for; matrix products, arithmetic and copies ran while one was open for 1% of the time, Pallas kernels for 0%

commit v1 on v0

--- a/solution.py
+++ b/solution.py
@@ -6,6 +6,12 @@
 D = 2048
 HEAD_DIM = 128
 norm_epsilon = 1e-06
+
+
+def gather_and_add(x, axis):
+    shards = lax.all_gather(x, axis, axis=0, tiled=False)
+    total = shards.sum(axis=0)
+    return total
 
 
 def unit_rows(vector):
@@ -125,7 +131,7 @@
         ],
         axis=1,
     )
-    gate_up = lax.psum(summand.astype(jnp.bfloat16), "tp").astype(jnp.float32)
+    gate_up = gather_and_add(summand.astype(jnp.bfloat16), "tp").astype(jnp.float32)
     gate_up = gate_up * mid_scale[:, None]
     activated = (jax.nn.silu(gate_up[:, :hidden_dev]) * gate_up[:, hidden_dev:]).astype(
         jnp.bfloat16

time: 165 us -> 147 us (0.89)
  waiting for transfers between devices: 65.3 us -> 46 us
  blocking collectives: 57.3 us -> 59.4 us
    psum x1 -> x0, waiting for transfers between devices: 16.3 us -> none  [local(): gate_up = lax.psum(summand.astype(jnp.bfloat16), 'tp').astype(jnp.float32)]
    reduce_scatter x1, waiting for transfers between devices: 20.7 us -> 17.6 us  [local(): lax.psum_scatter(down_local.astype(jnp.bfloat16), 'kv', scatter_dimension...]
    all_gather x0 -> x1, blocking collectives: none -> 2.06 us  [gather_and_add(): shards = lax.all_gather(x, axis, axis=0, tiled=False)]
    unnamed x5 -> x4, waiting for transfers between devices: 20.8 us -> 20.8 us
  transfers between devices with their start and end apart: 4 -> 3, of which waited for: 4 -> 3; matrix products, arithmetic and copies ran while one was open for 1% -> 1% of each run, Pallas kernels for 0% -> 0%
where the time goes in v1:
time: 147 us; the launch traced here: 146 us
  blocking collectives  59.4 us (40%)
  waiting for transfers between devices  46 us (31%)
  matrix products  17 us (12%)
  between operations  14.6 us (10%)
  other arithmetic  5.56 us (4%)
  local copies, waits for them, and re-layouts  3.14 us (2%)
    unnamed x4, waiting for transfers between devices  20.8 us
    reduce_scatter x1, waiting for transfers between devices, local(): lax.psum_scatter(down_local.astype(jnp.bfloat16), 'kv', scatter_dimension...  17.6 us
    psum x1, blocking collectives, local(): square_total = lax.psum(jnp.sum(square_pair, axis=1), 'kv')  13.3 us
    all_gather x1, blocking collectives, local(): lax.all_gather(normed_own, 'kv', axis=1, tiled=True)  13.3 us
    all_gather x1, blocking collectives, local(): lax.all_gather(mixed, 'kv', axis=0, tiled=True)  13.1 us
    all_gather x1, blocking collectives, local(): lax.all_gather(mid_squares.astype(jnp.bfloat16), 'kv', axis=1, tiled=True)  11.1 us
    reduce_scatter x1, waiting for transfers between devices, local(): lax.psum_scatter(attn_part.astype(jnp.bfloat16), 'tp', scatter_dimension=...  7.59 us
    dot_general x6, matrix products, local(): jnp.dot(row_block, weight, preferred_element_type=jnp.float32)  6.6 us
  transfers between devices with their start and end apart: 3, of which 3 were waited for; matrix products, arithmetic and copies ran while one was open for 1% of the time, Pallas kernels for 0%

profile of v1, /device:TPU:0, one launch (start us, length us, event | category | flops | bytes accessed | tf_op | source)
XLA Modules:
  0.0 145.9 jit_solution(14273505552138581751)
XLA Ops:
  7.3 0.8 convert_element_type.101
  8.1 2.3 %all_gather.19 = bf16[32,512]{1,0:T(8,128)(2,1)S(1)} all-gather(bf16[32,256]{1,0:T(8,128)(2,1)} %param.16), channel_id=1, replica_groups=mesh['dp'=4,'kv'=4,'tp'=2] {'tp'}, dimensions={1}, use_global_device_ids=true | all-gather | bytes 49152 | tf_op jit(solution)/shard_map/all_gather | solution.py:75
  11.2 0.8 convolution_convert_fusion.8
  12.3 1.2 convolution_convert_fusion.6
  13.5 1.2 convolution_convert_fusion.5
  14.7 1.2 convolution_convert_fusion.4
  16.0 1.2 convolution_convert_fusion.7
  18.2 1.8 %all-gather = bf16[2,1,32]{2,1,0:T(2,128)(2,1)S(1)} all-gather(bf16[1,1,32]{2,1,0:T(2,128)(2,1)S(1)} %bitcast.76), channel_id=1, replica_groups=mesh['dp'=4,'kv'=4,'tp'=2] {'tp'}, dimensions={0}, use_global_device_ids=true | all-gather | bytes 192 | tf_op jit(solution)/shard_map/all_gather | solution.py:76
  20.0 13.3 %psum.14 = f32[32]{0:T(128)S(1)} all-reduce(f32[32]{0:T(128)S(1)} %convert_reduce_fusion.1), channel_id=1, replica_groups=mesh['dp'=4,'kv'=4,'tp'=2] {'kv'}, use_global_device_ids=true, to_apply=%region_3.0 | all-reduce | flops 32 | bytes 256 | tf_op jit(solution)/shard_map/psum | solution.py:80
  34.7 20.7 %all-reduce.3.cloned.1.call-done = bf16[32,2056]{1,0:T(8,128)(2,1)} async-done(((bf16[32,2056]{1,0:T(8,128)(2,1)}), bf16[32,2056]{1,0:T(8,128)(2,1)}) %all-reduce.3.cloned.1.call-update) | async-done | bytes 131600
  55.4 0.8 convert_multiply_fusion.1
  56.7 3.6 %fusion.18 = f32[8,4,1,128]{3,2,1,0:T(1,128)S(1)} fusion(f32[8,4,128,128]{3,2,1,0:T(8,128)} %param.17, f32[8,4,128,1]{2,0,1,3:T(8,128)S(1)} %bitcast.74), kind=kOutput, calls=%fused_computation.45 | convolution fusion | flops 6291456 | bytes 2129920 | tf_op jit(solution)/shard_map/bhkv,bhk->bhv/dot_general | solution.py:32
  61.1 1.3 copy-done.2
  62.4 1.9 %fusion.16 = f32[8,4,1,128]{3,2,1,0:T(1,128)S(1)} fusion(f32[8,4,128,128]{3,2,1,0:T(8,128)S(1)} %multiply_add_fusion, f32[8,4,128,1]{2,0,1,3:T(8,128)S(1)} %get-tuple-element.4), kind=kOutput, calls=%fused_computation.43 | convolution fusion | flops 6291456 | bytes 2129920 | tf_op jit(solution)/shard_map/bhkv,bhk->bhv/dot_general | solution.py:37
  64.5 13.1 %all_gather.21 = bf16[32,512]{1,0:T(8,128)(2,1)S(1)} all-gather(bf16[8,512]{1,0:T(8,128)(2,1)S(1)} %fusion.20), channel_id=1, replica_groups=mesh['dp'=4,'kv'=4,'tp'=2] {'kv'}, dimensions={0}, use_global_device_ids=true | all-gather | bytes 40960 | tf_op jit(solution)/shard_map/all_gather | solution.py:107
  78.6 7.6 %reduce-scatter.3.cloned.1.call-done = bf16[32,256]{1,0:T(8,128)(2,1)} async-done(((bf16[32,512]{1,0:T(8,128)(2,1)}), bf16[32,256]{1,0:T(8,128)(2,1)}) %reduce-scatter.3.cloned.1.call-update) | async-done | bytes 16400 | tf_op jit(solution)/shard_map/reduce_scatter | solution.py:109
  86.2 0.8 fusion.8
  87.0 11.1 %all-gather.1 = bf16[4,1,32]{2,1,0:T(2,128)(2,1)S(1)} all-gather(bf16[1,1,32]{2,1,0:T(2,128)(2,1)S(1)} %bitcast.75), channel_id=1, replica_groups=mesh['dp'=4,'kv'=4,'tp'=2] {'kv'}, dimensions={0}, use_global_device_ids=true | all-gather | bytes 320 | tf_op jit(solution)/shard_map/all_gather | solution.py:119
  98.1 2.5 %psum.15 = f32[32]{0:T(128)S(1)} all-reduce(f32[32]{0:T(128)S(1)} %convert_reduce_fusion), channel_id=1, replica_groups=mesh['dp'=4,'kv'=4,'tp'=2] {'tp'}, use_global_device_ids=true, to_apply=%region_11.12 | all-reduce | flops 32 | bytes 256 | tf_op jit(solution)/shard_map/psum | solution.py:123
  100.6 13.3 %all_gather.22 = bf16[32,1024]{1,0:T(8,128)(2,1)S(1)} all-gather(bf16[32,256]{1,0:T(8,128)(2,1)S(1)} %get-tuple-element.9), channel_id=1, replica_groups=mesh['dp'=4,'kv'=4,'tp'=2] {'kv'}, dimensions={1}, use_global_device_ids=true | all-gather | bytes 81920 | tf_op jit(solution)/shard_map/all_gather | solution.py:118
  115.1 2.1 %all_gather.23 = bf16[2,32,2816]{2,1,0:T(8,128)(2,1)S(1)} all-gather(bf16[1,32,2816]{2,1,0:T(8,128)(2,1)S(1)} %pad_maximum_fusion), channel_id=1, replica_groups=mesh['dp'=4,'kv'=4,'tp'=2] {'tp'}, dimensions={0}, use_global_device_ids=true | all-gather | bytes 540672 | tf_op jit(solution)/shard_map/all_gather | solution.py:12
  117.3 3.0 %convolution_convert_fusion.2 = bf16[32,1024]{1,0:T(8,128)(2,1)} fusion(bf16[1408,1024]{1,0:T(8,128)(2,1)} %param.31, f32[32,2816]{1,0:T(8,128)S(1)} %convert_multiply_fusion), kind=kOutput, calls=%fused_computation.5 | convolution fusion | flops 92577792 | bytes 3309568 | tf_op jit(solution)/shard_map/dot_general | solution.py:139
  120.4 17.6 %reduce-scatter.5.cloned.1.call-done = bf16[32,256]{1,0:T(8,128)(2,1)} async-done(((bf16[32,1024]{1,0:T(8,128)(2,1)}), bf16[32,256]{1,0:T(8,128)(2,1)}) %reduce-scatter.5.cloned.1.call-update) | async-done | bytes 16400 | tf_op jit(solution)/shard_map/reduce_scatter | solution.py:140
  138.0 1.3 fusion.9
  (59 shorter events, 6.6 us)
Async XLA Ops:
  7.2 106.7 %copy-start = (bf16[1024,1408]{1,0:T(8,128)(2,1)S(1)}, bf16[1024,1408]{1,0:T(8,128)(2,1)}, u32[]{:S(2)}) copy-start(bf16[1024,1408]{1,0:T(8,128)(2,1)} %param.30) | copy-start | bytes 8650756
  7.2 26.2 %copy-start.10 = (u32[32]{0:T(128)S(1)}, u32[32]{0:T(128)}, u32[]{:S(2)}) copy-start(u32[32]{0:T(128)} %constant.50) | copy-start | bytes 388
  7.2 10.9 %copy-start.5 = (bf16[32,256]{1,0:T(8,128)(2,1)S(1)}, bf16[32,256]{1,0:T(8,128)(2,1)}, u32[]{:S(2)}) copy-start(bf16[32,256]{1,0:T(8,128)(2,1)} %param.16) | copy-start | bytes 49156
  7.2 11.0 %copy-start.9 = (f32[4]{0:T(128)S(1)}, f32[4]{0:T(128)}, u32[]{:S(2)}) copy-start(f32[4]{0:T(128)} %param.25) | copy-start | bytes 52
  7.2 48.2 %all-reduce.3.cloned.1.call-start = ((), (), s32[]{:S(2)}) async-start(), calls=%async_computation.4 | async-start | bytes 278528
  18.0 68.2 %reduce-scatter.3.cloned.1.call-start = ((), (), s32[]{:S(2)}) async-start(), calls=%async_computation.2 | async-start | bytes 49152 | tf_op jit(solution)/shard_map/reduce_scatter | solution.py:109
  56.6 3.8 %copy-start.1 = (f32[8,4,128,128]{3,2,1,0:T(8,128)S(1)}, f32[8,4,128,128]{3,2,1,0:T(8,128)}, u32[]{:S(2)}) copy-start(f32[8,4,128,128]{3,2,1,0:T(8,128)} %param.17) | copy-start | bytes 6291460
  61.1 1.3 copy-start.2
  61.1 3.3 %copy-start.7 = (f32[128]{0:T(128)S(1)}, f32[128]{0:T(128)}, u32[]{:S(2)}) copy-start(f32[128]{0:T(128)} %param.26) | copy-start | bytes 1540
  61.1 16.5 %copy-start.4 = (bf16[512,512]{1,0:T(8,128)(2,1)S(1)}, bf16[512,512]{1,0:T(8,128)(2,1)}, u32[]{:S(2)}) copy-start(bf16[512,512]{1,0:T(8,128)(2,1)} %param.27) | copy-start | bytes 1572868
  61.1 17.4 %copy-start.8 = (bf16[512]{0:T(512)(128)(2,1)S(1)}, bf16[512]{0:T(512)(128)(2,1)}, u32[]{:S(2)}) copy-start(bf16[512]{0:T(512)(128)(2,1)} %param.28) | copy-start | bytes 3076
  78.5 59.6 %reduce-scatter.5.cloned.1.call-start = ((), (), s32[]{:S(2)}) async-start(), calls=%async_computation.3 | async-start | bytes 81920 | tf_op jit(solution)/shard_map/reduce_scatter | solution.py:140
  100.6 13.9 %copy-start.3 = (bf16[1024,1408]{1,0:T(8,128)(2,1)S(1)}, bf16[1024,1408]{1,0:T(8,128)(2,1)}, u32[]{:S(2)}) copy-start(bf16[1024,1408]{1,0:T(8,128)(2,1)} %param.29) | copy-start | bytes 8650756
  117.1 20.9 %copy-start.6 = (bf16[32,256]{1,0:T(8,128)(2,1)S(1)}, bf16[32,256]{1,0:T(8,128)(2,1)}, u32[]{:S(2)}) copy-start(bf16[32,256]{1,0:T(8,128)(2,1)} %reduce-scatter.3.cloned.1.call-done) | copy-start | bytes 49156
Sparse Core Ops, SparseCore 0:
  18.1 37.2 all-reduce.2
  78.6 7.5 reduce-scatter.2
  120.5 17.4 reduce-scatter.4
